TPU v7x, 32 devices: a whole 2x2x4 slice. The times are simulated.
32 devices in a mesh: sp: 16 (over z, y, x), tp: 2 (over core).
Axes of the slice: x: 2, y: 2, z: 4, core: 2. Of those that a mesh axis runs over, the one named last changes fastest.
Arguments:
- stream: bfloat16 [4096, 2048], P(('sp', 'tp')), may hold values from -6 to 6
- queries: bfloat16 [4096, 1024], P('sp', 'tp'), may hold values from -6 to 6
- keys_in: bfloat16 [4096, 1024], P('sp', 'tp'), may hold values from -6 to 6
- values_in: bfloat16 [4096, 1024], P('sp', 'tp'), may hold values from -6 to 6
- gate_in: bfloat16 [4096, 1024], P('sp', 'tp'), may hold values from -6 to 6
- log_decay: float32 [4096, 8], P('sp', 'tp'), may hold values from -0.8 to 0
- head_gain: bfloat16 [1024], P('tp'), may hold values from 0.099609375 to 1.8984375
- out_weight: bfloat16 [1024, 2048], P('tp'), may hold values from -0.1875 to 0.1875
- norm_gain: bfloat16 [2048], replicated, may hold values from 0.099609375 to 1.8984375
- gate_weight: bfloat16 [2048, 5632], P('sp', 'tp'), may hold values from -0.125 to 0.125
- up_weight: bfloat16 [2048, 5632], P('sp', 'tp'), may hold values from -0.125 to 0.125
- down_weight: bfloat16 [5632, 2048], P('tp', 'sp'), may hold values from -0.078125 to 0.078125
Outputs:
- result: bfloat16 [4096, 2048], P(('sp', 'tp'))
All inputs are finite; a program needn't handle non-finite values.
Results may differ from a plain program's by a relative error of at most 0.02.
Values may be sent and summed in bfloat16 or wider, within the bound.
A program may use at most 128 MiB of HBM per device.

v0:
```python
import jax
import jax.numpy as jnp
from jax import lax
from jax.sharding import PartitionSpec as P

BLOCK = 128
epsilon = 1e-06
highest = lax.Precision.HIGHEST


def carried_in(value, axis, combine, identity):
    length, here = (lax.axis_size(axis), lax.axis_index(axis))
    everything = jax.tree.map(
        lambda part, kind: lax.all_gather(part.astype(kind), axis),
        value,
        (jnp.bfloat16, jnp.bfloat16),
    )
    start = jax.tree.map(
        lambda part, zero: jnp.broadcast_to(jnp.asarray(zero, part.dtype), part.shape),
        value,
        identity,
    )

    def turn(k, before):
        reached = k < here
        new = combine(
            before, jax.tree.map(lambda part, own: part[k].astype(own.dtype), everything, value)
        )
        return jax.tree.map(lambda a, b: jnp.where(reached, a, b), new, before)

    return lax.fori_loop(0, length, turn, start)


def block_pass(state, block_inputs):
    query_block, key_block, value_block, decay_block = block_inputs
    head_dim = query_block.shape[-1]
    key_scale = head_dim ** (-0.5)
    running = jnp.cumsum(decay_block, axis=0)
    scores = (
        jnp.einsum("ihd,jhd->hij", query_block, key_block, preferred_element_type=jnp.float32)
        * key_scale
    )
    offsets = jnp.arange(decay_block.shape[0])
    causal = offsets[:, None] >= offsets[None, :]
    log_gap = running.T[:, :, None] - running.T[:, None, :]
    decay_table = jnp.where(causal[None], jnp.exp(jnp.minimum(log_gap, 0.0)), 0.0)
    value_wide = value_block.astype(jnp.float32)
    within = jnp.einsum("hij,jhe->ihe", scores * decay_table, value_wide, precision=highest)
    query_wide = query_block.astype(jnp.float32) * jnp.exp(running)[:, :, None]
    carried = jnp.einsum("ihd,hde->ihe", query_wide, state, precision=highest)
    block_total = running[-1]
    key_wide = (
        key_block.astype(jnp.float32) * key_scale * jnp.exp(block_total[None] - running)[:, :, None]
    )
    state = jnp.exp(block_total)[:, None, None] * state + jnp.einsum(
        "jhd,jhe->hde", key_wide, value_wide, precision=highest
    )
    return (state, within + carried)


def chain_combine(earlier_pair, later_pair):
    return (
        earlier_pair[0] * later_pair[0],
        later_pair[0][:, None, None] * earlier_pair[1] + later_pair[1],
    )


def local(
    stream,
    queries,
    keys_in,
    values_in,
    gate_in,
    log_decay,
    head_gain,
    out_weight,
    norm_gain,
    gate_weight,
    up_weight,
    down_weight,
):
    gate_full, up_full = (
        lax.all_gather(gate_weight, "sp", axis=0, tiled=True),
        lax.all_gather(up_weight, "sp", axis=0, tiled=True),
    )
    down_full = lax.all_gather(down_weight, "sp", axis=1, tiled=True)
    row_count, heads_here = log_decay.shape
    head_dim = queries.shape[1] // heads_here
    block_count = row_count // BLOCK
    block_shape = (block_count, BLOCK, heads_here, head_dim)
    block_inputs = (
        queries.reshape(block_shape),
        keys_in.reshape(block_shape),
        values_in.reshape(block_shape),
        log_decay.reshape(block_count, BLOCK, heads_here),
    )
    start_state = jnp.zeros((heads_here, head_dim, head_dim), jnp.float32)
    final_state, within = lax.scan(block_pass, start_state, block_inputs)
    within = within.reshape(row_count, heads_here, head_dim)
    running = jnp.cumsum(log_decay, axis=0)
    device_total = running[-1]
    scanned = carried_in(
        (jnp.exp(device_total), final_state),
        "sp",
        chain_combine,
        (jnp.ones_like(device_total), jnp.zeros_like(final_state)),
    )
    incoming = scanned[1]
    query_wide = (
        queries.reshape(row_count, heads_here, head_dim).astype(jnp.float32)
        * jnp.exp(running)[:, :, None]
    )
    retained = within + jnp.einsum("ihd,hde->ihe", query_wide, incoming, precision=highest)
    center = jnp.mean(retained, axis=-1, keepdims=True)
    spread = jnp.mean(jnp.square(retained - center), axis=-1, keepdims=True)
    normed_heads = (
        (retained - center)
        * lax.rsqrt(spread + epsilon)
        * head_gain.astype(jnp.float32).reshape(heads_here, head_dim)
    )
    mixed = (
        jax.nn.silu(gate_in.astype(jnp.float32))
        * normed_heads.reshape(row_count, heads_here * head_dim)
    ).astype(jnp.bfloat16)
    attended = lax.psum_scatter(
        jnp.dot(mixed, out_weight, preferred_element_type=jnp.float32).astype(jnp.bfloat16),
        "tp",
        scatter_dimension=0,
        tiled=True,
    ).astype(jnp.float32)
    residual = stream.astype(jnp.float32) + attended
    normed = (
        residual
        * lax.rsqrt(jnp.mean(residual * residual, axis=-1, keepdims=True) + epsilon)
        * norm_gain.astype(jnp.float32)
    ).astype(jnp.bfloat16)
    whole_rows = lax.all_gather(normed, "tp", axis=0, tiled=True)
    gate_sum = jnp.dot(whole_rows, gate_full, preferred_element_type=jnp.float32)
    up_sum = jnp.dot(whole_rows, up_full, preferred_element_type=jnp.float32)
    hidden = (jax.nn.silu(gate_sum) * up_sum).astype(jnp.bfloat16)
    down_terms = jnp.dot(hidden, down_full, preferred_element_type=jnp.float32)
    mixer_out = lax.psum_scatter(
        down_terms.astype(jnp.bfloat16), "tp", scatter_dimension=0, tiled=True
    ).astype(jnp.float32)
    return (residual + mixer_out).astype(jnp.bfloat16)


def solution(mesh):
    return jax.shard_map(
        local,
        mesh=mesh,
        in_specs=(
            P(("sp", "tp"), None),
            P("sp", "tp"),
            P("sp", "tp"),
            P("sp", "tp"),
            P("sp", "tp"),
            P("sp", "tp"),
            P("tp"),
            P("tp", None),
            P(),
            P("sp", "tp"),
            P("sp", "tp"),
            P("tp", "sp"),
        ),
        out_specs=P(("sp", "tp"), None),
        check_vma=False,
    )
```

profile of v0, /device:TPU:0, one launch (start us, length us, event | category | flops | bytes accessed | tf_op | source)
XLA Modules:
  0.0 643.5 jit_solution(10230276023747323382)
XLA Ops:
  6.5 1.9 reshape.105
  8.4 1.7 reshape.106
  10.1 1.7 reshape.107
  11.8 0.8 copy.97
  12.7 24.1 %while.27 = (s32[]{:T(128)}, f32[4,128,128]{2,1,0:T(8,128)S(1)}, f32[2,128,4,128]{1,0,3,2:T(2,128)}, f32[2,128,4]{2,1,0:T(8,128)S(1)}, bf16[2,128,4,128]{3,2,1,0...) while((s32[]{:T(128)}, f32[4,128,128]{2,1,0:T(8,128)S(1)}, ...), condition=%wide.region_2.3_spmd.clone, body=%wide.region_0.2_spmd.clone.sunk | while | flops 319767040 | bytes 4260068 | solution.py:98
  12.7 1.1 constant_dynamic-slice_fusion.6
  13.8 0.2 reduce_window_sum.31
  14.0 1.0 constant_dynamic-slice_fusion.5
  15.0 0.2 fusion.56
  15.2 0.4 convolution_bitcast_fusion.4
  15.7 0.7 fusion.57
  16.5 7.7 %dynamic_update_slice.6 = f32[2,128,4,128]{1,0,3,2:T(2,128)} dynamic-update-slice(f32[2,128,4,128]{1,0,3,2:T(2,128)} %get-tuple-element.359, f32[1,128,4,128]{1,0,3,2:T(1,128)S(1)} %bitcast.115, s32[]{:T(128)} %get-tuple-element.357, s32[]{:T(128)} %constant.67.clone.1..sunk, s32[]{:T(128)} %constant.67.clone.1..sunk, s32[]{:T(128)} %constant.67.clone.1..sunk) | dynamic-update-slice | bytes 524292 | tf_op jit(solution)/shard_map/while/body/jit(dynamic_update_index_in_dim)/dynamic_update_slice | solution.py:98
  24.2 0.5 convolution_add_fusion.2
  24.7 1.1 constant_dynamic-slice_fusion.6
  25.8 0.2 reduce_window_sum.31
  26.0 1.0 constant_dynamic-slice_fusion.5
  27.0 0.2 fusion.56
  27.3 0.4 convolution_bitcast_fusion.4
  27.8 0.7 fusion.57
  28.5 7.7 %dynamic_update_slice.6 = f32[2,128,4,128]{1,0,3,2:T(2,128)} dynamic-update-slice(f32[2,128,4,128]{1,0,3,2:T(2,128)} %get-tuple-element.359, f32[1,128,4,128]{1,0,3,2:T(1,128)S(1)} %bitcast.115, s32[]{:T(128)} %get-tuple-element.357, s32[]{:T(128)} %constant.67.clone.1..sunk, s32[]{:T(128)} %constant.67.clone.1..sunk, s32[]{:T(128)} %constant.67.clone.1..sunk) | dynamic-update-slice | bytes 524292 | tf_op jit(solution)/shard_map/while/body/jit(dynamic_update_index_in_dim)/dynamic_update_slice | solution.py:98
  36.2 0.5 convolution_add_fusion.2
  36.8 0.7 convert_element_type.81
  37.5 1.2 reduce-window.6
  38.8 0.1 copy.102
  39.2 0.2 fusion.26
  39.3 42.5 %all-gather.1 = bf16[16,1,4]{2,1,0:T(2,128)(2,1)S(1)} all-gather(bf16[1,1,4]{2,1,0:T(2,128)(2,1)S(1)} %bitcast.124), channel_id=1, replica_groups=mesh['sp'=16,'tp'=2] {'sp'}, dimensions={0}, use_global_device_ids=true | all-gather | bytes 136 | tf_op jit(solution)/shard_map/all_gather | solution.py:14
  82.0 1.5 reshape.108
  83.5 17.2 %all-gather.16.cloned.1.call-done = bf16[64,128,128]{2,1,0:T(8,128)(2,1)} async-done(((bf16[4,128,128]{2,1,0:T(8,128)(2,1)}), bf16[64,128,128]{2,1,0:T(8,128)(2,1)}) %all-gather.16.cloned.1.call-update) | async-done | bytes 2097168 | tf_op jit(solution)/shard_map/all_gather | solution.py:14
  100.7 16.8 %while.28 = (s32[]{:T(128)}, f32[4,128,128]{2,1,0:T(8,128)S(1)}, s32[]{:T(128)}, bf16[16,4]{1,0:T(8,128)(2,1)S(1)}, bf16[16,4,128,128]{3,2,1,0:T(8,128)(2,1)}, /*index=5*/s32[]{:T(128)}, s32[]{:T(128)}) while((s32[]{:T(128)}, f32[4,128,128]{2,1,0:T(8,128)S(1)}, s32[]{:T(128)}, bf16[16,4]{1,0:T(8,128)(2,1)S(1)}, ...), condition=%wide.region_6.7_spmd.clone, body=%wide.region_5.6_spmd.clone.sunk | while | flops 327688 | bytes 655505 | solution.py:31
  100.7 1.0 fusion.58
  101.7 1.0 fusion.58
  102.8 1.0 fusion.58
  103.8 1.0 fusion.58
  104.9 1.0 fusion.58
  105.9 1.0 fusion.58
  107.0 1.0 fusion.58
  108.1 1.0 fusion.58
  109.1 1.0 fusion.58
  110.2 1.0 fusion.58
  111.2 1.0 fusion.58
  112.3 1.0 fusion.58
  113.3 1.0 fusion.58
  114.4 1.0 fusion.58
  115.4 1.0 fusion.58
  116.5 1.0 fusion.58
  117.5 0.8 fusion.31
  118.4 0.1 multiply_multiply_fusion
  118.6 0.2 copy.108
  118.8 1.7 convolution_convert_fusion.1
  120.6 7.3 %reduce-scatter.3.cloned.1.call-done = bf16[128,2048]{1,0:T(8,128)(2,1)} async-done(((bf16[256,2048]{1,0:T(8,128)(2,1)}), bf16[128,2048]{1,0:T(8,128)(2,1)}) %reduce-scatter.3.cloned.1.call-update) | async-done | bytes 524304 | tf_op jit(solution)/shard_map/reduce_scatter | solution.py:125
  127.9 1.3 multiply_reduce_fusion
  129.2 2.0 multiply_convert_fusion
  131.3 0.5 all-gather.10.cloned.1.call-update
  131.9 0.5 all-gather.12.cloned.1.call-update
  132.5 0.5 all-gather.14.cloned.1.call-update
  133.0 0.2 reduce-scatter.5.cloned.1.call-start
  133.3 8.4 %all-gather.8.cloned.1.call-done = bf16[256,2048]{1,0:T(8,128)(2,1)} async-done(((bf16[128,2048]{1,0:T(8,128)(2,1)}), bf16[256,2048]{1,0:T(8,128)(2,1)}) %all-gather.8.cloned.1.call-update) | async-done | bytes 1048592 | tf_op jit(solution)/shard_map/all_gather | solution.py:137
  141.7 145.2 %all-gather.10.cloned.1.call-done = bf16[2048,2816]{1,0:T(8,128)(2,1)} async-done(((bf16[128,2816]{1,0:T(8,128)(2,1)}), bf16[2048,2816]{1,0:T(8,128)(2,1)}) %all-gather.10.cloned.1.call-update) | async-done | bytes 11534352 | tf_op jit(solution)/shard_map/all_gather | solution.py:83
  286.9 9.4 %fusion.32 = f32[256,2816]{1,0:T(8,128)} fusion(bf16[256,2048]{1,0:T(8,128)(2,1)} %all-gather.8.cloned.1.call-done, bf16[2048,2816]{1,0:T(8,128)(2,1)} %all-gather.10.cloned.1.call-done), kind=kOutput, calls=%fused_computation.68 | convolution fusion | flops 2952790016 | bytes 15466496 | tf_op jit(solution)/shard_map/dot_general | solution.py:138
  296.3 132.8 %all-gather.12.cloned.1.call-done = bf16[2048,2816]{1,0:T(8,128)(2,1)} async-done(((bf16[128,2816]{1,0:T(8,128)(2,1)}), bf16[2048,2816]{1,0:T(8,128)(2,1)}) %all-gather.12.cloned.1.call-update) | async-done | bytes 11534352 | tf_op jit(solution)/shard_map/all_gather | solution.py:84
  429.2 182.8 %all-gather.14.cloned.1.call-done = bf16[2816,2048]{1,0:T(8,128)(2,1)} async-done(((bf16[2816,128]{1,0:T(8,128)(2,1)}), bf16[2816,2048]{1,0:T(8,128)(2,1)}) %all-gather.14.cloned.1.call-update) | async-done | bytes 11534352 | tf_op jit(solution)/shard_map/all_gather | solution.py:86
  612.0 15.9 %convolution_convert_fusion = bf16[256,2048]{1,0:T(8,128)(2,1)} fusion(bf16[2816,2048]{1,0:T(8,128)(2,1)} %all-gather.14.cloned.1.call-done, bf16[256,2048]{1,0:T(8,128)(2,1)} %all-gather.8.cloned.1.call-done, bf16[2048,2816]{1,0:T(8,128)(2,1)} %all-gather.12.cloned.1.call-done, f32[256,2816]{1,0:T(8,128)} %fusion.32), kind=kOutput, calls=%fused_computation.32 | convolution fusion | flops 5910429696 | bytes 28049408 | tf_op jit(solution)/shard_map/dot_general | solution.py:141
  627.9 6.7 %reduce-scatter.5.cloned.1.call-done = bf16[128,2048]{1,0:T(8,128)(2,1)} async-done(((bf16[256,2048]{1,0:T(8,128)(2,1)}), bf16[128,2048]{1,0:T(8,128)(2,1)}) %reduce-scatter.5.cloned.1.call-update) | async-done | bytes 524304 | tf_op jit(solution)/shard_map/reduce_scatter | solution.py:142
  634.6 2.1 add_convert_fusion
  (77 shorter events, 1.6 us)
Async XLA Ops:
  6.5 112.2 %copy-start = (bf16[512,2048]{1,0:T(8,128)(2,1)S(1)}, bf16[512,2048]{1,0:T(8,128)(2,1)}, u32[]{:S(2)}) copy-start(bf16[512,2048]{1,0:T(8,128)(2,1)} %param.23) | copy-start | bytes 6291460
  6.5 94.1 %all-gather.16.cloned.1.call-start = ((), (), s32[]{:S(2)}) async-start(), calls=%async_computation.8 | async-start | bytes 2228224 | tf_op jit(solution)/shard_map/all_gather | solution.py:14
  12.6 24.9 %copy-start.4 = (f32[256,4]{0,1:T(4,128)S(1)}, f32[256,4]{0,1:T(4,128)}, u32[]{:S(2)}) copy-start(f32[256,4]{0,1:T(4,128)} %param.21) | copy-start | bytes 12292
  12.7 70.8 %copy-start.6 = (bf16[512]{0:T(512)(128)(2,1)S(1)}, bf16[512]{0:T(512)(128)(2,1)}, u32[]{:S(2)}) copy-start(bf16[512]{0:T(512)(128)(2,1)} %param.22) | copy-start | bytes 3076
  36.7 80.8 %copy-start.3 = (bf16[256,512]{1,0:T(8,128)(2,1)S(1)}, bf16[256,512]{1,0:T(8,128)(2,1)}, u32[]{:S(2)}) copy-start(bf16[256,512]{1,0:T(8,128)(2,1)} %param.17) | copy-start | bytes 786436
  37.4 90.5 %reduce-scatter.3.cloned.1.call-start = ((), (), s32[]{:S(2)}) async-start(), calls=%async_computation.2 | async-start | bytes 1572864 | tf_op jit(solution)/shard_map/reduce_scatter | solution.py:125
  117.5 1.3 copy-start.7
  118.8 1.8 copy-start.5
  118.8 9.1 %copy-start.1 = (bf16[128,2048]{1,0:T(8,128)(2,1)S(1)}, bf16[128,2048]{1,0:T(8,128)(2,1)}, u32[]{:S(2)}) copy-start(bf16[128,2048]{1,0:T(8,128)(2,1)} %param.16) | copy-start | bytes 1572868
  120.6 21.1 %all-gather.8.cloned.1.call-start = ((), (), s32[]{:S(2)}) async-start(), calls=%async_computation.3 | async-start | bytes 1572864 | tf_op jit(solution)/shard_map/all_gather | solution.py:137
  131.3 155.6 %all-gather.10.cloned.1.call-start = ((), (), s32[]{:S(2)}) async-start(), calls=%async_computation.4 | async-start | bytes 12255232 | tf_op jit(solution)/shard_map/all_gather | solution.py:83
  131.9 297.3 %all-gather.12.cloned.1.call-start = ((), (), s32[]{:S(2)}) async-start(), calls=%async_computation.5 | async-start | bytes 12255232 | tf_op jit(solution)/shard_map/all_gather | solution.py:84
  132.5 479.5 %all-gather.14.cloned.1.call-start = ((), (), s32[]{:S(2)}) async-start(), calls=%async_computation.6 | async-start | bytes 12255232 | tf_op jit(solution)/shard_map/all_gather | solution.py:86
  133.0 501.6 %reduce-scatter.5.cloned.1.call-start = ((), (), s32[]{:S(2)}) async-start(), calls=%async_computation.7 | async-start | bytes 1572864 | tf_op jit(solution)/shard_map/reduce_scatter | solution.py:142
  296.3 338.3 %copy-start.2 = (bf16[128,2048]{1,0:T(8,128)(2,1)S(1)}, bf16[128,2048]{1,0:T(8,128)(2,1)}, u32[]{:S(2)}) copy-start(bf16[128,2048]{1,0:T(8,128)(2,1)} %reduce-scatter.3.cloned.1.call-done) | copy-start | bytes 1572868
Sparse Core Ops, SparseCore 0:
  37.6 63.0 all-gather.15
  120.7 7.1 reduce-scatter.2
  131.4 10.2 all-gather.7
  144.3 142.5 all-gather.9
  289.5 139.5 all-gather.11
  431.7 180.2 all-gather.13
  628.0 6.5 reduce-scatter.4
where the time goes:
time: 645 us; the launch traced here: 644 us
  waiting for transfers between devices  502 us (78%)
  blocking collectives  42.5 us (7%)
  matrix products  31.5 us (5%)
  local copies, waits for them, and re-layouts  28.1 us (4%)
  other arithmetic  24.6 us (4%)
  between operations  13.7 us (2%)
    all_gather x1, waiting for transfers between devices, local(): down_full = lax.all_gather(down_weight, 'sp', axis=1, tiled=True)  183 us
    all_gather x1, waiting for transfers between devices, local(): lax.all_gather(gate_weight, 'sp', axis=0, tiled=True)  145 us
    all_gather x1, waiting for transfers between devices, local(): lax.all_gather(up_weight, 'sp', axis=0, tiled=True)  133 us
    all_gather x1, blocking collectives, carried_in(): lax.all_gather(part.astype(kind), axis)  42.5 us
    all_gather x1, waiting for transfers between devices, carried_in(): lax.all_gather(part.astype(kind), axis)  17.2 us
    select_n x16, other arithmetic, turn(): return jax.tree.map(lambda a, b: jnp.where(reached, a, b), new, before)  16.2 us
    dot_general x1, matrix products, local(): down_terms = jnp.dot(hidden, down_full, preferred_element_type=jnp.float32)  15.9 us
    dynamic_update_slice x2, local copies, waits for them, and re-layouts, local(): final_state, within = lax.scan(block_pass, start_state, block_inputs)  15.3 us
  transfers between devices with their start and end apart: 7, of which 7 were waited for; matrix products, arithmetic and copies ran while one was open for 2% of the time, Pallas kernels for 0%

commit v1 on v0

--- a/solution.py
+++ b/solution.py
@@ -1,3 +1,4 @@
+import functools
 import jax
 import jax.numpy as jnp
 from jax import lax
@@ -6,6 +7,13 @@
 BLOCK = 128
 epsilon = 1e-06
 highest = lax.Precision.HIGHEST
+
+
+def _open_page(xs, axis_id, d0):
+    return jnp.concatenate(lax.all_gather(xs, axis_id), axis=d0)
+
+
+match_the_sheets = functools.partial(_open_page, axis_id="sp", d0=1)
 
 
 def carried_in(value, axis, combine, identity):
@@ -83,7 +91,7 @@
         lax.all_gather(gate_weight, "sp", axis=0, tiled=True),
         lax.all_gather(up_weight, "sp", axis=0, tiled=True),
     )
-    down_full = lax.all_gather(down_weight, "sp", axis=1, tiled=True)
+    down_full = match_the_sheets(down_weight)
     row_count, heads_here = log_decay.shape
     head_dim = queries.shape[1] // heads_here
     block_count = row_count // BLOCK

time: 645 us -> 603 us (0.935)
  waiting for transfers between devices: 502 us -> 445 us
  local copies, waits for them, and re-layouts: 28.1 us -> 43.2 us
    all_gather x1, waiting for transfers between devices: 183 us -> 141 us  [_open_page(): return jnp.concatenate(lax.all_gather(xs, axis_id), axis=d0)]
    reshape x1 -> x2, local copies, waits for them, and re-layouts: 0.01 us -> 15.1 us  [the longest x1 15.1 us: _open_page(): return jnp.concatenate(lax.all_gather(xs, axis_id), axis=d0)]
    all_gather x1, waiting for transfers between devices: 8.44 us -> 0.01 us  [local(): whole_rows = lax.all_gather(normed, 'tp', axis=0, tiled=True)]
    all_gather x1, waiting for transfers between devices: 145 us -> 139 us  [local(): lax.all_gather(gate_weight, 'sp', axis=0, tiled=True)]
  transfers between devices with their start and end apart: 7 -> 7, of which waited for: 7 -> 6; matrix products, arithmetic and copies ran while one was open for 2% -> 5% of each run, Pallas kernels for 0% -> 0%
where the time goes in v1:
time: 603 us; the launch traced here: 601 us
  waiting for transfers between devices  445 us (74%)
  local copies, waits for them, and re-layouts  43.2 us (7%)
  blocking collectives  42.5 us (7%)
  matrix products  31.5 us (5%)
  other arithmetic  24.6 us (4%)
  between operations  13.7 us (2%)
    all_gather x1, waiting for transfers between devices, _open_page(): return jnp.concatenate(lax.all_gather(xs, axis_id), axis=d0)  141 us
    all_gather x1, waiting for transfers between devices, local(): lax.all_gather(gate_weight, 'sp', axis=0, tiled=True)  139 us
    all_gather x1, waiting for transfers between devices, local(): lax.all_gather(up_weight, 'sp', axis=0, tiled=True)  133 us
    all_gather x1, blocking collectives, carried_in(): lax.all_gather(part.astype(kind), axis)  42.5 us
    all_gather x1, waiting for transfers between devices, carried_in(): lax.all_gather(part.astype(kind), axis)  17.2 us
    select_n x16, other arithmetic, turn(): return jax.tree.map(lambda a, b: jnp.where(reached, a, b), new, before)  16.2 us
    dot_general x1, matrix products, local(): down_terms = jnp.dot(hidden, down_full, preferred_element_type=jnp.float32)  15.9 us
    dynamic_update_slice x2, local copies, waits for them, and re-layouts, local(): final_state, within = lax.scan(block_pass, start_state, block_inputs)  15.3 us
  transfers between devices with their start and end apart: 7, of which 6 were waited for; matrix products, arithmetic and copies ran while one was open for 5% of the time, Pallas kernels for 0%

profile of v1, /device:TPU:0, one launch (start us, length us, event | category | flops | bytes accessed | tf_op | source)
XLA Modules:
  0.0 601.1 jit_solution(17356322570436744122)
XLA Ops:
  6.5 1.9 reshape.111
  8.4 1.7 reshape.112
  10.1 1.7 reshape.113
  11.8 0.8 copy.121
  12.7 24.1 %while.27 = (s32[]{:T(128)}, f32[4,128,128]{2,1,0:T(8,128)S(1)}, f32[2,128,4,128]{1,0,3,2:T(2,128)}, f32[2,128,4]{2,1,0:T(8,128)S(1)}, bf16[2,128,4,128]{3,2,1,0...) while((s32[]{:T(128)}, f32[4,128,128]{2,1,0:T(8,128)S(1)}, ...), condition=%wide.region_2.3_spmd.clone, body=%wide.region_0.2_spmd.clone.sunk | while | flops 319767040 | bytes 4260068 | solution.py:106
  12.7 1.1 constant_dynamic-slice_fusion.6
  13.8 0.2 reduce_window_sum.31
  14.0 1.0 constant_dynamic-slice_fusion.5
  15.0 0.2 fusion.56
  15.2 0.4 convolution_bitcast_fusion.4
  15.8 0.7 fusion.57
  16.5 7.7 %dynamic_update_slice.6 = f32[2,128,4,128]{1,0,3,2:T(2,128)} dynamic-update-slice(f32[2,128,4,128]{1,0,3,2:T(2,128)} %get-tuple-element.371, f32[1,128,4,128]{1,0,3,2:T(1,128)S(1)} %bitcast.119, s32[]{:T(128)} %get-tuple-element.369, s32[]{:T(128)} %constant.67.clone.1..sunk, s32[]{:T(128)} %constant.67.clone.1..sunk, s32[]{:T(128)} %constant.67.clone.1..sunk) | dynamic-update-slice | bytes 524292 | tf_op jit(solution)/shard_map/while/body/jit(dynamic_update_index_in_dim)/dynamic_update_slice | solution.py:106
  24.2 0.5 convolution_add_fusion.2
  24.7 1.1 constant_dynamic-slice_fusion.6
  25.8 0.2 reduce_window_sum.31
  26.1 1.0 constant_dynamic-slice_fusion.5
  27.1 0.2 fusion.56
  27.3 0.4 convolution_bitcast_fusion.4
  27.8 0.7 fusion.57
  28.5 7.7 %dynamic_update_slice.6 = f32[2,128,4,128]{1,0,3,2:T(2,128)} dynamic-update-slice(f32[2,128,4,128]{1,0,3,2:T(2,128)} %get-tuple-element.371, f32[1,128,4,128]{1,0,3,2:T(1,128)S(1)} %bitcast.119, s32[]{:T(128)} %get-tuple-element.369, s32[]{:T(128)} %constant.67.clone.1..sunk, s32[]{:T(128)} %constant.67.clone.1..sunk, s32[]{:T(128)} %constant.67.clone.1..sunk) | dynamic-update-slice | bytes 524292 | tf_op jit(solution)/shard_map/while/body/jit(dynamic_update_index_in_dim)/dynamic_update_slice | solution.py:106
  36.2 0.5 convolution_add_fusion.2
  36.8 0.7 convert_element_type.81
  37.6 1.2 reduce-window.6
  38.9 0.1 copy.126
  39.2 0.2 fusion.26
  39.4 42.5 %all-gather.2 = bf16[16,1,4]{2,1,0:T(2,128)(2,1)S(1)} all-gather(bf16[1,1,4]{2,1,0:T(2,128)(2,1)S(1)} %bitcast.130), channel_id=1, replica_groups=mesh['sp'=16,'tp'=2] {'sp'}, dimensions={0}, use_global_device_ids=true | all-gather | bytes 136 | tf_op jit(solution)/shard_map/all_gather | solution.py:22
  82.0 1.5 reshape.114
  83.5 17.2 %all-gather.15.cloned.1.call-done = bf16[64,128,128]{2,1,0:T(8,128)(2,1)} async-done(((bf16[4,128,128]{2,1,0:T(8,128)(2,1)}), bf16[64,128,128]{2,1,0:T(8,128)(2,1)}) %all-gather.15.cloned.1.call-update) | async-done | bytes 2097168 | tf_op jit(solution)/shard_map/all_gather | solution.py:22
  100.7 16.8 %while.28 = (s32[]{:T(128)}, f32[4,128,128]{2,1,0:T(8,128)S(1)}, s32[]{:T(128)}, bf16[16,4]{1,0:T(8,128)(2,1)S(1)}, bf16[16,4,128,128]{3,2,1,0:T(8,128)(2,1)}, /*index=5*/s32[]{:T(128)}, s32[]{:T(128)}) while((s32[]{:T(128)}, f32[4,128,128]{2,1,0:T(8,128)S(1)}, s32[]{:T(128)}, bf16[16,4]{1,0:T(8,128)(2,1)S(1)}, ...), condition=%wide.region_6.7_spmd.clone, body=%wide.region_5.6_spmd.clone.sunk | while | flops 327688 | bytes 655505 | solution.py:39
  100.7 1.0 fusion.58
  101.8 1.0 fusion.58
  102.8 1.0 fusion.58
  103.9 1.0 fusion.58
  104.9 1.0 fusion.58
  106.0 1.0 fusion.58
  107.0 1.0 fusion.58
  108.1 1.0 fusion.58
  109.1 1.0 fusion.58
  110.2 1.0 fusion.58
  111.2 1.0 fusion.58
  112.3 1.0 fusion.58
  113.3 1.0 fusion.58
  114.4 1.0 fusion.58
  115.5 1.0 fusion.58
  116.5 1.0 fusion.58
  117.6 0.8 fusion.31
  118.5 0.1 multiply_multiply_fusion
  118.6 0.2 copy.132
  118.8 1.7 convolution_convert_fusion.1
  120.7 0.7 all-gather.17.cloned.1.call-update
  121.4 6.5 %reduce-scatter.3.cloned.1.call-done = bf16[128,2048]{1,0:T(8,128)(2,1)} async-done(((bf16[256,2048]{1,0:T(8,128)(2,1)}), bf16[128,2048]{1,0:T(8,128)(2,1)}) %reduce-scatter.3.cloned.1.call-update) | async-done | bytes 524304 | tf_op jit(solution)/shard_map/reduce_scatter | solution.py:133
  128.0 1.3 multiply_reduce_fusion
  129.3 2.0 multiply_convert_fusion
  131.4 0.5 all-gather.11.cloned.1.call-update
  132.0 0.5 all-gather.13.cloned.1.call-update
  132.5 0.2 reduce-scatter.5.cloned.1.call-start
  132.7 140.7 %all-gather.17.cloned.1.call-done = bf16[45056,128]{1,0:T(8,128)(2,1)} async-done(((bf16[2816,128]{1,0:T(8,128)(2,1)}), bf16[45056,128]{1,0:T(8,128)(2,1)}) %all-gather.17.cloned.1.call-update) | async-done | bytes 11534352 | tf_op jit(solution)/shard_map/all_gather | solution.py:13
  273.4 15.1 %copy.133 = bf16[2816,16,128]{0,2,1:T(8,128)(2,1)} copy(bf16[2816,16,128]{2,0,1:T(8,128)(2,1)} %bitcast.121) | data formatting | bytes 23068672 | tf_op jit(solution)/shard_map/reshape | solution.py:13
  288.5 138.7 %all-gather.11.cloned.1.call-done = bf16[2048,2816]{1,0:T(8,128)(2,1)} async-done(((bf16[128,2816]{1,0:T(8,128)(2,1)}), bf16[2048,2816]{1,0:T(8,128)(2,1)}) %all-gather.11.cloned.1.call-update) | async-done | bytes 11534352 | tf_op jit(solution)/shard_map/all_gather | solution.py:91
  427.3 9.4 %fusion.32 = f32[256,2816]{1,0:T(8,128)} fusion(bf16[256,2048]{1,0:T(8,128)(2,1)} %all-gather.9.cloned.1.call-done, bf16[2048,2816]{1,0:T(8,128)(2,1)} %all-gather.11.cloned.1.call-done), kind=kOutput, calls=%fused_computation.68 | convolution fusion | flops 2952790016 | bytes 15466496 | tf_op jit(solution)/shard_map/dot_general | solution.py:146
  436.6 132.9 %all-gather.13.cloned.1.call-done = bf16[2048,2816]{1,0:T(8,128)(2,1)} async-done(((bf16[128,2816]{1,0:T(8,128)(2,1)}), bf16[2048,2816]{1,0:T(8,128)(2,1)}) %all-gather.13.cloned.1.call-update) | async-done | bytes 11534352 | tf_op jit(solution)/shard_map/all_gather | solution.py:92
  569.5 15.9 %convolution_convert_fusion = bf16[256,2048]{1,0:T(8,128)(2,1)} fusion(bf16[2816,2048]{0,1:T(8,128)(2,1)} %bitcast.122, bf16[256,2048]{1,0:T(8,128)(2,1)} %all-gather.9.cloned.1.call-done, bf16[2048,2816]{1,0:T(8,128)(2,1)} %all-gather.13.cloned.1.call-done, f32[256,2816]{1,0:T(8,128)} %fusion.32), kind=kOutput, calls=%fused_computation.32 | convolution fusion | flops 5910429696 | bytes 28049408 | tf_op jit(solution)/shard_map/dot_general | solution.py:149
  585.5 6.7 %reduce-scatter.5.cloned.1.call-done = bf16[128,2048]{1,0:T(8,128)(2,1)} async-done(((bf16[256,2048]{1,0:T(8,128)(2,1)}), bf16[128,2048]{1,0:T(8,128)(2,1)}) %reduce-scatter.5.cloned.1.call-update) | async-done | bytes 524304 | tf_op jit(solution)/shard_map/reduce_scatter | solution.py:150
  592.2 2.1 add_convert_fusion
  (80 shorter events, 1.6 us)
Async XLA Ops:
  6.5 112.3 %copy-start = (bf16[512,2048]{1,0:T(8,128)(2,1)S(1)}, bf16[512,2048]{1,0:T(8,128)(2,1)}, u32[]{:S(2)}) copy-start(bf16[512,2048]{1,0:T(8,128)(2,1)} %param.23) | copy-start | bytes 6291460
  6.5 94.2 %all-gather.15.cloned.1.call-start = ((), (), s32[]{:S(2)}) async-start(), calls=%async_computation.7 | async-start | bytes 2228224 | tf_op jit(solution)/shard_map/all_gather | solution.py:22
  12.7 24.9 %copy-start.5 = (f32[256,4]{0,1:T(4,128)S(1)}, f32[256,4]{0,1:T(4,128)}, u32[]{:S(2)}) copy-start(f32[256,4]{0,1:T(4,128)} %param.21) | copy-start | bytes 12292
  12.7 70.8 %copy-start.7 = (bf16[512]{0:T(512)(128)(2,1)S(1)}, bf16[512]{0:T(512)(128)(2,1)}, u32[]{:S(2)}) copy-start(bf16[512]{0:T(512)(128)(2,1)} %param.22) | copy-start | bytes 3076
  36.8 80.8 %copy-start.4 = (bf16[256,512]{1,0:T(8,128)(2,1)S(1)}, bf16[256,512]{1,0:T(8,128)(2,1)}, u32[]{:S(2)}) copy-start(bf16[256,512]{1,0:T(8,128)(2,1)} %param.17) | copy-start | bytes 786436
  37.5 90.5 %reduce-scatter.3.cloned.1.call-start = ((), (), s32[]{:S(2)}) async-start(), calls=%async_computation.2 | async-start | bytes 1572864 | tf_op jit(solution)/shard_map/reduce_scatter | solution.py:133
  117.5 1.3 copy-start.8
  118.8 2.6 copy-start.6
  118.8 9.1 %copy-start.2 = (bf16[128,2048]{1,0:T(8,128)(2,1)S(1)}, bf16[128,2048]{1,0:T(8,128)(2,1)}, u32[]{:S(2)}) copy-start(bf16[128,2048]{1,0:T(8,128)(2,1)} %param.16) | copy-start | bytes 1572868
  120.6 152.8 %all-gather.17.cloned.1.call-start = ((), (), s32[]{:S(2)}) async-start(), calls=%async_computation.8 | async-start | bytes 12255232 | tf_op jit(solution)/shard_map/all_gather | solution.py:13
  121.3 167.2 %all-gather.9.cloned.1.call-start = ((), (), s32[]{:S(2)}) async-start(), calls=%async_computation.3 | async-start | bytes 1572864 | tf_op jit(solution)/shard_map/all_gather | solution.py:145
  131.3 295.9 %all-gather.11.cloned.1.call-start = ((), (), s32[]{:S(2)}) async-start(), calls=%async_computation.4 | async-start | bytes 12255232 | tf_op jit(solution)/shard_map/all_gather | solution.py:91
  131.9 437.6 %all-gather.13.cloned.1.call-start = ((), (), s32[]{:S(2)}) async-start(), calls=%async_computation.5 | async-start | bytes 12255232 | tf_op jit(solution)/shard_map/all_gather | solution.py:92
  132.5 459.7 %reduce-scatter.5.cloned.1.call-start = ((), (), s32[]{:S(2)}) async-start(), calls=%async_computation.6 | async-start | bytes 1572864 | tf_op jit(solution)/shard_map/reduce_scatter | solution.py:150
  569.5 22.7 %copy-start.3 = (bf16[128,2048]{1,0:T(8,128)(2,1)S(1)}, bf16[128,2048]{1,0:T(8,128)(2,1)}, u32[]{:S(2)}) copy-start(bf16[128,2048]{1,0:T(8,128)(2,1)} %reduce-scatter.3.cloned.1.call-done) | copy-start | bytes 1572868
  569.5 24.8 %copy-start.1 = (bf16[512,2048]{1,0:T(8,128)(2,1)S(1)}, bf16[512,2048]{1,0:T(8,128)(2,1)}, u32[]{:S(2)}) copy-start(bf16[512,2048]{1,0:T(8,128)(2,1)} %param.23) | copy-start | bytes 6291460
Sparse Core Ops, SparseCore 0:
  37.6 63.0 all-gather.14
  120.7 7.1 reduce-scatter.2
  130.7 142.6 all-gather.16
  274.8 7.1 all-gather.8
  284.6 142.5 all-gather.10
  429.9 139.5 all-gather.12
  585.6 6.5 reduce-scatter.4
